TPU v7x, 32 devices: a whole 2x2x4 slice. The times are simulated.
32 devices in a mesh: ep: 4 (over y, x), tp: 8 (over z, core).
Axes of the slice: x: 2, y: 2, z: 4, core: 2. Of those that a mesh axis runs over, the one named last changes fastest.
Arguments:
- queries: bfloat16 [2048, 16, 128], P('ep', 'tp'), may hold values from -125 to 125
- keys: bfloat16 [2048, 16, 128], P('ep', 'tp'), may hold values from -9 to 9
- values: bfloat16 [2048, 16, 128], P('ep', 'tp'), may hold values from -6 to 6
- mixing: float32 [16], P('tp'), may hold values from 0.3 to 0.8
- head_gain: float32 [128], replicated, may hold values from 0.1 to 1.9
- out_weight: bfloat16 [16, 128, 2048], P('tp'), may hold values from -0.125 to 0.125
- tokens_b: bfloat16 [4096, 2048], P(('ep', 'tp')), may hold values from -6 to 6
- norm_gain: float32 [2048], replicated, may hold values from 0.1 to 1.9
- expert_ids: int32 [4096, 2], P(('ep', 'tp')), may hold values from 0 to 3, all different within a row; in each aligned block of 128 rows (0 to 127, 128 to 255, ...) at most 96 rows name the same one
- group_gate: float32 [4096], P(('ep', 'tp')), may hold values from 0.2 to 1
- expert_gate: float32 [4096, 2], P(('ep', 'tp')), may hold values from 0.1 to 0.9
- gate_weight: bfloat16 [4, 2048, 1024], P('ep', None, 'tp'), may hold values from -0.125 to 0.125
- up_weight: bfloat16 [4, 2048, 1024], P('ep', None, 'tp'), may hold values from -0.125 to 0.125
- down_weight: bfloat16 [4, 2048, 1024], P('ep', None, 'tp'), may hold values from -0.1875 to 0.1875
Outputs:
- mixed: bfloat16 [2048, 2048], P(('ep', 'tp'))
- routed: bfloat16 [4096, 2048], P(('ep', 'tp'))
Inputs may be any that keep to these rules, and one draw needn't show every extreme that they name: `expert_ids`: within each aligned block of 128 rows, no expert is named by more than 96 rows, and some block has an expert named by exactly 96 rows.
All inputs are finite; a program needn't handle non-finite values.
Results may differ from a plain program's by a relative error of at most 0.019.
Values may be sent and summed in bfloat16 or wider, within the bound.
A program may use at most 192 MiB of HBM per device.

v0:
```python
import math
import jax
import jax.numpy as jnp
from jax import lax
from jax.sharding import PartitionSpec as P

HEAD = 64


def attend_heads(queries, keys, values, mixing, head_gain):
    shard_rows = queries.shape[0]
    head_count = queries.shape[1]
    value_width = values.shape[2]
    query_start = lax.axis_index("ep") * shard_rows
    score_scale = 1.0 / math.sqrt(HEAD)
    query_pos = query_start + lax.iota(jnp.int32, shard_rows)

    def update(running, key_block, value_block, block_start):
        key_pos = block_start + lax.iota(jnp.int32, shard_rows)
        allowed = key_pos[None, :] <= query_pos[:, None]
        fresh = []
        for map_index in range(2):
            maximum, row_sum, numerator = running[3 * map_index : 3 * map_index + 3]
            offset = map_index * HEAD
            scores = (
                jnp.einsum(
                    "qhd,khd->hqk",
                    queries[:, :, offset : offset + HEAD],
                    key_block[:, :, offset : offset + HEAD],
                    preferred_element_type=jnp.float32,
                )
                * score_scale
            )
            scores = jnp.where(allowed[None], scores, -1e30)
            newmax = jnp.maximum(maximum, jnp.max(scores, axis=2))
            shrink = jnp.exp(maximum - newmax)
            weights = jnp.exp(scores - newmax[:, :, None])
            row_sum = row_sum * shrink + jnp.sum(weights, axis=2)
            numerator = numerator * shrink[:, :, None] + jnp.einsum(
                "hqk,khe->hqe",
                weights.astype(jnp.bfloat16),
                value_block,
                preferred_element_type=jnp.float32,
            )
            fresh += [newmax, row_sum, numerator]
        return tuple(fresh)

    floor_max = jnp.full((head_count, shard_rows), -1e30, jnp.float32)
    zero_sum = jnp.zeros((head_count, shard_rows), jnp.float32)
    zero_acc = jnp.zeros((head_count, shard_rows, value_width), jnp.float32)
    start_state = (floor_max, zero_sum, zero_acc, floor_max, zero_sum, zero_acc)
    running = start_state
    key_piece = lax.all_gather(keys, "ep", axis=0, tiled=True)
    value_piece = lax.all_gather(values, "ep", axis=0, tiled=True)
    blocks = key_piece.shape[0] // shard_rows
    key_blocks = key_piece.reshape(blocks, shard_rows, head_count, key_piece.shape[2])
    value_blocks = value_piece.reshape(blocks, shard_rows, head_count, value_width)

    def visit_block(state, inputs):
        key_block, value_block, block_index = inputs
        block_start = block_index * shard_rows
        state = lax.cond(
            block_start <= query_start + shard_rows - 1,
            lambda state_in: update(state_in, key_block, value_block, block_start),
            lambda state_in: state_in,
            state,
        )
        return (state, None)

    running, unused = lax.scan(
        visit_block, running, (key_blocks, value_blocks, lax.iota(jnp.int32, blocks))
    )
    state = running
    diff = state[2] / state[1][:, :, None] - mixing[:, None, None] * state[5] / state[4][:, :, None]
    normed = diff * lax.rsqrt(jnp.mean(diff * diff, axis=2, keepdims=True) + 1e-05) * head_gain
    return normed.astype(jnp.bfloat16)


def mixer_half(queries, keys, values, mixing, head_gain, out_weight):
    attended = attend_heads(queries, keys, values, mixing, head_gain)
    return lax.psum_scatter(
        jnp.einsum("hqe,hed->qd", attended, out_weight, preferred_element_type=jnp.float32).astype(
            jnp.bfloat16
        ),
        "tp",
        scatter_dimension=0,
        tiled=True,
    )


def expert_half(
    tokens_b, norm_gain, expert_ids, group_gate, expert_gate, gate_weight, up_weight, down_weight
):
    local_rows = tokens_b.shape[0]
    width = tokens_b.shape[1]
    top_count = expert_ids.shape[1]
    ep_count = lax.axis_size("ep")
    local_count = gate_weight.shape[0]
    expert_total = ep_count * local_count
    capacity = 3 * local_rows * top_count // (2 * expert_total)
    tokens_f = tokens_b.astype(jnp.float32)
    normed = (
        tokens_f
        * lax.rsqrt(jnp.mean(tokens_f * tokens_f, axis=1, keepdims=True) + 1e-06)
        * norm_gain
    ).astype(jnp.bfloat16)
    flat_ids = expert_ids.reshape(-1)
    one_hot = (flat_ids[:, None] == lax.iota(jnp.int32, expert_total)[None, :]).astype(jnp.int32)
    slot_rank = jnp.sum((jnp.cumsum(one_hot, axis=0) - one_hot) * one_hot, axis=1)
    slot_index = flat_ids * capacity + slot_rank
    owners = jnp.full((expert_total * capacity,), local_rows, jnp.int32)
    owners = owners.at[slot_index].set(lax.iota(jnp.int32, local_rows * top_count) // top_count)
    padded = jnp.concatenate([normed, jnp.zeros((1, width), jnp.bfloat16)], axis=0)
    outgoing = padded[owners].reshape(ep_count, local_count * capacity, width)
    incoming = lax.all_to_all(outgoing, "ep", split_axis=0, concat_axis=0, tiled=True)
    expert_rows = jnp.transpose(
        incoming.reshape(ep_count, local_count, capacity, width), (1, 0, 2, 3)
    )
    expert_rows = expert_rows.reshape(local_count, ep_count * capacity, width)
    piece_gate = lax.all_gather(gate_weight, "tp", axis=2, tiled=True)
    piece_up = lax.all_gather(up_weight, "tp", axis=2, tiled=True)
    piece_down = lax.all_gather(down_weight, "tp", axis=2, tiled=True)
    gate_part = jnp.einsum(
        "jrd,jdf->jrf", expert_rows, piece_gate, preferred_element_type=jnp.float32
    )
    up_part = jnp.einsum("jrd,jdf->jrf", expert_rows, piece_up, preferred_element_type=jnp.float32)
    hidden = (jax.nn.silu(gate_part) * up_part).astype(jnp.bfloat16)
    expert_out = jnp.einsum(
        "jrf,jdf->jrd", hidden, piece_down, preferred_element_type=jnp.float32
    ).astype(jnp.bfloat16)
    outbound = jnp.transpose(
        expert_out.reshape(local_count, ep_count, capacity, width), (1, 0, 2, 3)
    )
    outbound = outbound.reshape(ep_count, local_count * capacity, width)
    returned = lax.all_to_all(outbound, "ep", split_axis=0, concat_axis=0, tiled=True).reshape(
        expert_total * capacity, width
    )
    picked = returned[slot_index].reshape(local_rows, top_count, width).astype(jnp.float32)
    route_weight = group_gate[:, None] * expert_gate
    return jnp.sum(route_weight[:, :, None] * picked, axis=1).astype(jnp.bfloat16)


def per_device(
    queries,
    keys,
    values,
    mixing,
    head_gain,
    out_weight,
    tokens_b,
    norm_gain,
    expert_ids,
    group_gate,
    expert_gate,
    gate_weight,
    up_weight,
    down_weight,
):
    mixed = mixer_half(queries, keys, values, mixing, head_gain, out_weight)
    routed = expert_half(
        tokens_b,
        norm_gain,
        expert_ids,
        group_gate,
        expert_gate,
        gate_weight,
        up_weight,
        down_weight,
    )
    return (mixed, routed)


def solution(mesh):
    placed = (
        P("ep", "tp", None),
        P("ep", "tp", None),
        P("ep", "tp", None),
        P("tp"),
        P(),
        P("tp", None, None),
        P(("ep", "tp"), None),
        P(),
        P(("ep", "tp"), None),
        P(("ep", "tp")),
        P(("ep", "tp"), None),
        P("ep", None, "tp"),
        P("ep", None, "tp"),
        P("ep", None, "tp"),
    )
    return jax.shard_map(
        per_device,
        mesh=mesh,
        in_specs=placed,
        out_specs=(P(("ep", "tp"), None), P(("ep", "tp"), None)),
        check_vma=False,
    )
```

profile of v0, /device:TPU:0, one launch (start us, length us, event | category | flops | bytes accessed | tf_op | source)
XLA Modules:
  0.0 260.2 jit_solution(6079203360803837472)
XLA Ops:
  7.3 1.8 copy.24
  9.1 1.7 copy.25
  13.4 1.2 reduce-window.6
  15.3 1.4 scatter_custom_fusion
  17.0 1.0 fusion.33
  17.9 21.8 %all-gather.6.cloned.1.call-done = bf16[2048,2,128]{2,0,1:T(8,128)(2,1)} async-done(((bf16[512,2,128]{2,0,1:T(8,128)(2,1)}), bf16[2048,2,128]{2,0,1:T(8,128)(2,1)}) %all-gather.6.cloned.1.call-update) | async-done | bytes 1048592 | tf_op jit(solution)/shard_map/all_gather | solution.py:53
  39.7 2.3 copy.26
  42.0 26.1 %all-gather.8.cloned.1.call-done = bf16[2048,2,128]{2,0,1:T(8,128)(2,1)} async-done(((bf16[512,2,128]{2,0,1:T(8,128)(2,1)}), bf16[2048,2,128]{2,0,1:T(8,128)(2,1)}) %all-gather.8.cloned.1.call-update) | async-done | bytes 1048592 | tf_op jit(solution)/shard_map/all_gather | solution.py:54
  68.1 1.3 copy.28
  69.5 9.8 %while.23 = (s32[]{:T(128)}, f32[2,512]{1,0:T(2,128)S(1)}, f32[2,512]{1,0:T(2,128)S(1)}, f32[2,512,128]{2,1,0:T(8,128)S(1)}, f32[2,512]{1,0:T(2,128)S(1)}, /*ind...) while((s32[]{:T(128)}, f32[2,512]{1,0:T(2,128)S(1)}, ...), condition=%wide.region_7.8_spmd.clone, body=%wide.region_0.7_spmd.clone.sunk | while | flops 410784768 | bytes 17183128 | solution.py:70
  70.8 4.6 %conditional.3 = ((f32[2,512]{1,0:T(2,128)S(1)}, f32[2,512]{1,0:T(2,128)S(1)}, f32[2,512,128]{2,1,0:T(8,128)S(1)}, f32[2,512]{1,0:T(2,128)S(1)}, f32[2,512]{1,0:T(2,128)S(1)}, /*index=5*/f32[2,512,128]{2,1,0:T(8,128)S(1)})) conditional(s32[]{:T(128)} %convert_element_type.87, (f32[2,512]{1,0:T(2,128)S(1)}, f32[2,512]{1,0:T(2,128)S(1)}, ...), branch_computations={%region_1.1_spmd, %region_2.6_spmd} | conditional | flops 410784768 | bytes 17180748 | solution.py:62
  70.8 1.0 dynamic-slice_bitcast_fusion
  79.9 2.1 bitcast_convert_fusion
  82.2 2.5 gather_fusion
  84.6 36.1 %all_to_all.10 = bf16[4,96,2048]{2,1,0:T(8,128)(2,1)} all-to-all(bf16[4,96,2048]{2,1,0:T(8,128)(2,1)S(1)} %bitcast.62), channel_id=1, replica_groups=mesh['ep'=4,'tp'=8] {'ep'}, dimensions={0} | all-to-all | bytes 3145728 | tf_op jit(solution)/shard_map/all_to_all | solution.py:115
  120.7 5.7 %fusion.24 = f32[384,1024]{1,0:T(8,128)} fusion(bf16[384,2048]{1,0:T(8,128)(2,1)} %bitcast.63, bf16[1,2048,1024]{2,1,0:T(8,128)(2,1)} %all-gather.10.cloned.1.call-done), kind=kOutput, calls=%fused_computation.38 | convolution fusion | flops 1610612736 | bytes 7340032 | tf_op jit(solution)/shard_map/jrd,jdf->jrf/dot_general | solution.py:123
  126.4 38.6 %all-gather.12.cloned.1.call-done = bf16[1,2048,1024]{2,1,0:T(8,128)(2,1)} async-done(((bf16[1,2048,128]{2,1,0:T(8,128)(2,1)}), bf16[1,2048,1024]{2,1,0:T(8,128)(2,1)}) %all-gather.12.cloned.1.call-update) | async-done | bytes 4194320 | tf_op jit(solution)/shard_map/all_gather | solution.py:121
  165.0 47.5 %all-gather.14.cloned.1.call-done = bf16[1,2048,1024]{2,1,0:T(8,128)(2,1)} async-done(((bf16[1,2048,128]{2,1,0:T(8,128)(2,1)}), bf16[1,2048,1024]{2,1,0:T(8,128)(2,1)}) %all-gather.14.cloned.1.call-update) | async-done | bytes 4194320 | tf_op jit(solution)/shard_map/all_gather | solution.py:122
  212.5 8.6 %fusion.26 = bf16[384,2048]{1,0:T(8,128)(2,1)} fusion(bf16[1,2048,1024]{2,1,0:T(8,128)(2,1)} %all-gather.14.cloned.1.call-done, f32[384,1024]{1,0:T(8,128)} %fusion.24, bf16[384,2048]{1,0:T(8,128)(2,1)S(1)} %bitcast.64, bf16[1,2048,1024]{2,1,0:T(8,128)(2,1)} %all-gather.12.cloned.1.call-done), kind=kOutput, calls=%fused_computation.41 | convolution fusion | flops 3224371200 | bytes 13107200 | tf_op jit(solution)/shard_map/jrf,jdf->jrd/dot_general | solution.py:128
  221.1 3.8 %all-to-all-start.1 = ((bf16[4,96,2048]{2,1,0:T(8,128)(2,1)}), bf16[4,96,2048]{2,1,0:T(8,128)(2,1)S(1)}, u32[]{:S(2)}, u32[]{:S(2)}) async-start(bf16[4,96,2048]{2,1,0:T(8,128)(2,1)} %bitcast.65), calls=%async_computation.2 | async-start | bytes 3145728 | tf_op jit(solution)/shard_map/all_to_all | solution.py:135
  225.0 19.7 %all-to-all-done.1 = bf16[4,96,2048]{2,1,0:T(8,128)(2,1)S(1)} async-done(((bf16[4,96,2048]{2,1,0:T(8,128)(2,1)}), bf16[4,96,2048]{2,1,0:T(8,128)(2,1)S(1)}, u32[]{:S(2)}, u32[]{:S(2)}) %all-to-all-start.1) | async-done | bytes 1572896 | tf_op jit(solution)/shard_map/all_to_all | solution.py:135
  244.7 2.3 gather_fusion.1
  247.1 2.4 reshape.163
  249.4 3.9 %multiply_reduce_fusion = bf16[128,2048]{1,0:T(8,128)(2,1)} fusion(f32[128,2,2048]{2,1,0:T(2,128)S(1)} %reshape.163, f32[128,2]{1,0:T(8,128)S(1)} %copy.29), kind=kLoop, calls=%fused_computation.42 | loop fusion | flops 786432 | bytes 2622464 | tf_op jit(solution)/shard_map/reduce_sum | solution.py:140
  (95 shorter events, 10.3 us)
Async XLA Ops:
  7.2 72.7 %copy-start = (bf16[2,128,2048]{2,1,0:T(8,128)(2,1)S(1)}, bf16[2,128,2048]{2,1,0:T(8,128)(2,1)}, u32[]{:S(2)}) copy-start(bf16[2,128,2048]{2,1,0:T(8,128)(2,1)} %param.23) | copy-start | bytes 3145732
  7.2 5.6 %copy-start.6 = (s32[128,2]{0,1:T(2,128)S(1)}, s32[128,2]{0,1:T(2,128)}, u32[]{:S(2)}) copy-start(s32[128,2]{0,1:T(2,128)} %param.26) | copy-start | bytes 3076
  7.2 6.0 %copy-start.4 = (bf16[512,2,128]{2,1,0:T(2,128)(2,1)S(1)}, bf16[512,2,128]{2,1,0:T(2,128)(2,1)}, u32[]{:S(2)}) copy-start(bf16[512,2,128]{2,1,0:T(2,128)(2,1)} %param.18) | copy-start | bytes 786436
  7.2 9.5 %copy-start.1 = (bf16[128,2048]{1,0:T(8,128)(2,1)S(1)}, bf16[128,2048]{1,0:T(8,128)(2,1)}, u32[]{:S(2)}) copy-start(bf16[128,2048]{1,0:T(8,128)(2,1)} %param.24) | copy-start | bytes 1572868
  7.2 32.5 %all-gather.6.cloned.1.call-start = ((), (), s32[]{:S(2)}) async-start(), calls=%async_computation.3 | async-start | bytes 1310720 | tf_op jit(solution)/shard_map/all_gather | solution.py:53
  9.1 7.9 %copy-start.5 = (f32[2048]{0:T(1024)S(1)}, f32[2048]{0:T(1024)}, u32[]{:S(2)}) copy-start(f32[2048]{0:T(1024)} %param.25) | copy-start | bytes 24580
  9.1 59.0 %all-gather.8.cloned.1.call-start = ((), (), s32[]{:S(2)}) async-start(), calls=%async_computation.4 | async-start | bytes 1310720 | tf_op jit(solution)/shard_map/all_gather | solution.py:54
  10.8 109.8 %all-gather.10.cloned.1.call-start = ((), (), s32[]{:S(2)}) async-start(), calls=%async_computation.6 | async-start | bytes 4718592 | tf_op jit(solution)/shard_map/all_gather | solution.py:120
  11.6 153.4 %all-gather.12.cloned.1.call-start = ((), (), s32[]{:S(2)}) async-start(), calls=%async_computation.7 | async-start | bytes 4718592 | tf_op jit(solution)/shard_map/all_gather | solution.py:121
  12.2 200.3 %all-gather.14.cloned.1.call-start = ((), (), s32[]{:S(2)}) async-start(), calls=%async_computation.8 | async-start | bytes 4718592 | tf_op jit(solution)/shard_map/all_gather | solution.py:122
  12.7 240.6 %reduce-scatter.2.cloned.1.call-start = ((), (), s32[]{:S(2)}) async-start(), calls=%async_computation.5 | async-start | bytes 2359296 | tf_op jit(solution)/shard_map/reduce_scatter | solution.py:81
  69.5 9.9 %copy-start.8 = (f32[2]{0:T(128)S(1)}, f32[2]{0:T(128)}, u32[]{:S(2)}) copy-start(f32[2]{0:T(128)} %param.21) | copy-start | bytes 28
  69.5 10.4 %copy-start.9 = (f32[128]{0:T(128)S(1)}, f32[128]{0:T(128)}, u32[]{:S(2)}) copy-start(f32[128]{0:T(128)} %param.22) | copy-start | bytes 1540
  79.9 2.2 copy-start.2
  120.7 91.8 %copy-start.3 = (bf16[4,96,2048]{2,1,0:T(8,128)(2,1)S(1)}, bf16[4,96,2048]{2,1,0:T(8,128)(2,1)}, u32[]{:S(2)}) copy-start(bf16[4,96,2048]{2,1,0:T(8,128)(2,1)} %all_to_all.10) | copy-start | bytes 4718596
  221.1 3.8 %copy-start.7 = (f32[128,2]{0,1:T(2,128)S(1)}, f32[128,2]{0,1:T(2,128)}, u32[]{:S(2)}) copy-start(f32[128,2]{0,1:T(2,128)} %param.28) | copy-start | bytes 3076
  221.1 3.8 %copy-start.10 = (f32[128]{0:T(128)S(1)}, f32[128]{0:T(128)}, u32[]{:S(2)}) copy-start(f32[128]{0:T(128)} %param.27) | copy-start | bytes 1540
  221.1 23.6 %all-to-all-start.1 = ((bf16[4,96,2048]{2,1,0:T(8,128)(2,1)}), bf16[4,96,2048]{2,1,0:T(8,128)(2,1)S(1)}, u32[]{:S(2)}, u32[]{:S(2)}) async-start(bf16[4,96,2048]{2,1,0:T(8,128)(2,1)} %bitcast.65), calls=%async_computation.2 | async-start | bytes 3145728 | tf_op jit(solution)/shard_map/all_to_all | solution.py:135
Sparse Core Ops, SparseCore 0:
  10.4 29.2 all-gather.5
  41.5 26.4 all-gather.7
  69.7 47.8 all-gather.9
  119.0 45.9 all-gather.11
  166.4 45.9 all-gather.13
  215.2 34.1 reduce-scatter.1
where the time goes:
time: 261 us; the launch traced here: 260 us
  waiting for transfers between devices  155 us (59%)
  blocking collectives  36.1 us (14%)
  local copies, waits for them, and re-layouts  20.4 us (8%)
  matrix products  19.2 us (7%)
  between operations  14.4 us (6%)
  other arithmetic  7.89 us (3%)
  starting transfers between devices  4.02 us (2%)
  loops' own time  2.93 us (1%)
    all_gather x1, waiting for transfers between devices, expert_half(): piece_down = lax.all_gather(down_weight, 'tp', axis=2, tiled=True)  47.5 us
    all_gather x1, waiting for transfers between devices, expert_half(): piece_up = lax.all_gather(up_weight, 'tp', axis=2, tiled=True)  38.6 us
    all_to_all x1, blocking collectives, expert_half(): lax.all_to_all(outgoing, 'ep', split_axis=0, concat_axis=0, tiled=True)  36.1 us
    all_gather x1, waiting for transfers between devices, attend_heads(): value_piece = lax.all_gather(values, 'ep', axis=0, tiled=True)  26.1 us
    all_gather x1, waiting for transfers between devices, attend_heads(): key_piece = lax.all_gather(keys, 'ep', axis=0, tiled=True)  21.8 us
    all_to_all x1, waiting for transfers between devices, expert_half(): lax.all_to_all(outbound, 'ep', split_axis=0, concat_axis=0, tiled=True)  19.7 us
    dot_general x1, matrix products, expert_half(): jnp.einsum('jrf,jdf->jrd', hidden, piece_down, preferred_element_type=jnp...  8.63 us
    unnamed x28, local copies, waits for them, and re-layouts  7.42 us
  transfers between devices with their start and end apart: 7, of which 5 were waited for; matrix products, arithmetic and copies ran while one was open for 18% of the time, Pallas kernels for 0%

commit v1 on v0

--- a/solution.py
+++ b/solution.py
@@ -5,6 +5,18 @@
 from jax.sharding import PartitionSpec as P
 
 HEAD = 64
+
+
+def product_in_turn(value, axis, dim, contribution):
+    size, here, width = (lax.axis_size(axis), lax.axis_index(axis), value.shape[dim])
+    right = [(i, (i + 1) % size) for i in range(size)]
+    held, total = (value, None)
+    for step in range(size):
+        coming = lax.ppermute(held, axis, right) if step < size - 1 else None
+        absorb = contribution(held, (here - step) % size * width)
+        total = absorb if total is None else total + absorb
+        held = coming
+    return total
 
 
 def attend_heads(queries, keys, values, mixing, head_gain):
@@ -119,14 +131,21 @@
     expert_rows = expert_rows.reshape(local_count, ep_count * capacity, width)
     piece_gate = lax.all_gather(gate_weight, "tp", axis=2, tiled=True)
     piece_up = lax.all_gather(up_weight, "tp", axis=2, tiled=True)
-    piece_down = lax.all_gather(down_weight, "tp", axis=2, tiled=True)
     gate_part = jnp.einsum(
         "jrd,jdf->jrf", expert_rows, piece_gate, preferred_element_type=jnp.float32
     )
     up_part = jnp.einsum("jrd,jdf->jrf", expert_rows, piece_up, preferred_element_type=jnp.float32)
     hidden = (jax.nn.silu(gate_part) * up_part).astype(jnp.bfloat16)
-    expert_out = jnp.einsum(
-        "jrf,jdf->jrd", hidden, piece_down, preferred_element_type=jnp.float32
+    expert_out = product_in_turn(
+        down_weight,
+        "tp",
+        2,
+        lambda own_block, offset_2: jnp.einsum(
+            "jrf,jdf->jrd",
+            lax.dynamic_slice_in_dim(hidden, offset_2, own_block.shape[2], axis=2),
+            own_block,
+            preferred_element_type=jnp.float32,
+        ),
     ).astype(jnp.bfloat16)
     outbound = jnp.transpose(
         expert_out.reshape(local_count, ep_count, capacity, width), (1, 0, 2, 3)

time: 261 us -> 238 us (0.912)
  blocking collectives: 36.1 us -> 0 us
  starting transfers between devices: 4.02 us -> 9.24 us
  matrix products: 19.2 us -> 24.3 us
  waiting for transfers between devices: 155 us -> 158 us
    ppermute x0 -> x7, waiting for transfers between devices: none -> 50 us  [product_in_turn(): coming = lax.ppermute(held, axis, right) if step < size - 1 else None]
    all_gather x1 -> x0, waiting for transfers between devices: 47.5 us -> none  [expert_half(): piece_down = lax.all_gather(down_weight, 'tp', axis=2, tiled=True)]
    all_to_all x1 -> x0, blocking collectives: 36.1 us -> none  [expert_half(): lax.all_to_all(outgoing, 'ep', split_axis=0, concat_axis=0, tiled=True)]
    all_gather x1, waiting for transfers between devices: 0.01 us -> 26.8 us  [expert_half(): piece_gate = lax.all_gather(gate_weight, 'tp', axis=2, tiled=True)]
    all_gather x1, waiting for transfers between devices: 21.8 us -> 0.02 us  [attend_heads(): key_piece = lax.all_gather(keys, 'ep', axis=0, tiled=True)]
    all_gather x1, waiting for transfers between devices: 26.1 us -> 19.9 us  [attend_heads(): value_piece = lax.all_gather(values, 'ep', axis=0, tiled=True)]
    dot_general x1 -> x9, matrix products: 8.63 us -> 13.8 us  [the longest x8 8.7 us: expert_half(): jnp.einsum('jrf,jdf->jrd', lax.dynamic_slice_in_dim(hidden, offset_2, own...]
    all_to_all x0 -> x1, starting transfers between devices: none -> 4.51 us  [expert_half(): lax.all_to_all(outgoing, 'ep', split_axis=0, concat_axis=0, tiled=True)]
  transfers between devices with their start and end apart: 7 -> 14, of which waited for: 5 -> 9; matrix products, arithmetic and copies ran while one was open for 18% -> 21% of each run, Pallas kernels for 0% -> 0%
where the time goes in v1:
time: 238 us
  waiting for transfers between devices  158 us (66%)
  matrix products  24.3 us (10%)
  local copies, waits for them, and re-layouts  21.9 us (9%)
  between operations  14.3 us (6%)
  starting transfers between devices  9.24 us (4%)
  other arithmetic  7.1 us (3%)
  loops' own time  2.92 us (1%)
    ppermute x7, waiting for transfers between devices, product_in_turn(): coming = lax.ppermute(held, axis, right) if step < size - 1 else None  50 us
    all_gather x1, waiting for transfers between devices, expert_half(): piece_up = lax.all_gather(up_weight, 'tp', axis=2, tiled=True)  40.3 us
    all_gather x1, waiting for transfers between devices, expert_half(): piece_gate = lax.all_gather(gate_weight, 'tp', axis=2, tiled=True)  26.8 us
    all_gather x1, waiting for transfers between devices, attend_heads(): value_piece = lax.all_gather(values, 'ep', axis=0, tiled=True)  19.9 us
    all_to_all x1, waiting for transfers between devices, expert_half(): lax.all_to_all(outbound, 'ep', split_axis=0, concat_axis=0, tiled=True)  19.6 us
    dot_general x8, matrix products, expert_half(): jnp.einsum('jrf,jdf->jrd', lax.dynamic_slice_in_dim(hidden, offset_2, own...  8.7 us
    unnamed x40, local copies, waits for them, and re-layouts  8.33 us
    dot_general x1, matrix products, expert_half(): jnp.einsum('jrd,jdf->jrf', expert_rows, piece_gate, preferred_element_typ...  5.69 us
  transfers between devices with their start and end apart: 14, of which 9 were waited for; matrix products, arithmetic and copies ran while one was open for 21% of the time, Pallas kernels for 0%

profile of v1, /device:TPU:0, one launch (start us, length us, event | category | flops | bytes accessed | tf_op | source)
XLA Modules:
  0.0 237.6 jit_solution(1039132844441037306)
XLA Ops:
  7.3 1.8 copy.24
  9.2 1.7 copy.25
  13.2 10.4 %collective-permute-done = bf16[1,2048,128]{2,1,0:T(8,128)(2,1)S(1)} collective-permute-done((bf16[1,2048,128]{2,1,0:T(8,128)(2,1)S(1)}, bf16[1,2048,128]{2,1,0:T(8,128)(2,1)S(1)}, u32[]{:S(2)}, u32[]{:S(2)}) %collective-permute-start) | collective-permute-done | bytes 524320 | tf_op jit(solution)/shard_map/ppermute | solution.py:15
  25.8 8.2 %collective-permute-done.1 = bf16[1,2048,128]{2,1,0:T(8,128)(2,1)S(1)} collective-permute-done((bf16[1,2048,128]{2,1,0:T(8,128)(2,1)S(1)}, bf16[1,2048,128]{2,1,0:T(8,128)(2,1)S(1)}, u32[]{:S(2)}, u32[]{:S(2)}) %collective-permute-start.1) | collective-permute-done | bytes 524320 | tf_op jit(solution)/shard_map/ppermute | solution.py:15
  34.1 10.3 %collective-permute-done.2 = bf16[1,2048,128]{2,1,0:T(8,128)(2,1)S(1)} collective-permute-done((bf16[1,2048,128]{2,1,0:T(8,128)(2,1)S(1)}, bf16[1,2048,128]{2,1,0:T(8,128)(2,1)S(1)}, u32[]{:S(2)}, u32[]{:S(2)}) %collective-permute-start.2) | collective-permute-done | bytes 524320 | tf_op jit(solution)/shard_map/ppermute | solution.py:15
  45.9 3.1 %gather_fusion = bf16[384,2048]{1,0:T(8,128)(2,1)} fusion(bf16[129,2048]{1,0:T(8,128)(2,1)S(1)} %concatenate.3, s32[1024]{0:T(1024)S(1)} %pad_clamp_fusion.1), kind=kCustom, calls=%fused_computation | custom fusion | bytes 3147264 | tf_op jit(solution)/shard_map/gather | solution.py:126
  49.0 4.5 %all-to-all-start = ((bf16[4,96,2048]{2,1,0:T(8,128)(2,1)}), bf16[4,96,2048]{2,1,0:T(8,128)(2,1)}, u32[]{:S(2)}, u32[]{:S(2)}) async-start(bf16[4,96,2048]{2,1,0:T(8,128)(2,1)} %bitcast.11), calls=%async_computation.1 | async-start | bytes 3145728 | tf_op jit(solution)/shard_map/all_to_all | solution.py:127
  55.2 2.3 copy.26
  57.5 19.9 %all-gather.7.cloned.1.call-done = bf16[2048,2,128]{2,0,1:T(8,128)(2,1)} async-done(((bf16[512,2,128]{2,0,1:T(8,128)(2,1)}), bf16[2048,2,128]{2,0,1:T(8,128)(2,1)}) %all-gather.7.cloned.1.call-update) | async-done | bytes 1048592 | tf_op jit(solution)/shard_map/all_gather | solution.py:66
  78.8 9.8 %while.23 = (s32[]{:T(128)}, f32[2,512]{1,0:T(2,128)S(1)}, f32[2,512]{1,0:T(2,128)S(1)}, f32[2,512,128]{2,1,0:T(8,128)S(1)}, f32[2,512]{1,0:T(2,128)S(1)}, /*ind...) while((s32[]{:T(128)}, f32[2,512]{1,0:T(2,128)S(1)}, ...), condition=%wide.region_7.8_spmd.clone, body=%wide.region_0.7_spmd.clone.sunk | while | flops 410784768 | bytes 17183128 | solution.py:82
  80.1 4.6 %conditional.3 = ((f32[2,512]{1,0:T(2,128)S(1)}, f32[2,512]{1,0:T(2,128)S(1)}, f32[2,512,128]{2,1,0:T(8,128)S(1)}, f32[2,512]{1,0:T(2,128)S(1)}, f32[2,512]{1,0:T(2,128)S(1)}, /*index=5*/f32[2,512,128]{2,1,0:T(8,128)S(1)})) conditional(s32[]{:T(128)} %convert_element_type.85, (f32[2,512]{1,0:T(2,128)S(1)}, f32[2,512]{1,0:T(2,128)S(1)}, ...), branch_computations={%region_1.1_spmd, %region_2.6_spmd} | conditional | flops 410784768 | bytes 17180748 | solution.py:74
  89.3 2.1 bitcast_convert_fusion
  91.5 19.8 %collective-permute-done.5 = bf16[1,2048,128]{2,1,0:T(8,128)(2,1)S(1)} collective-permute-done((bf16[1,2048,128]{2,1,0:T(8,128)(2,1)}, bf16[1,2048,128]{2,1,0:T(8,128)(2,1)S(1)}, u32[]{:S(2)}, u32[]{:S(2)}) %collective-permute-start.5) | collective-permute-done | bytes 524320 | tf_op jit(solution)/shard_map/ppermute | solution.py:15
  111.2 26.8 %all-gather.9.cloned.1.call-done = bf16[1,2048,1024]{2,1,0:T(8,128)(2,1)} async-done(((bf16[1,2048,128]{2,1,0:T(8,128)(2,1)}), bf16[1,2048,1024]{2,1,0:T(8,128)(2,1)}) %all-gather.9.cloned.1.call-update) | async-done | bytes 4194320 | tf_op jit(solution)/shard_map/all_gather | solution.py:132
  138.0 5.7 %fusion.22 = f32[384,1024]{1,0:T(8,128)} fusion(bf16[384,2048]{1,0:T(8,128)(2,1)} %bitcast.12, bf16[1,2048,1024]{2,1,0:T(8,128)(2,1)} %all-gather.9.cloned.1.call-done), kind=kOutput, calls=%fused_computation.36 | convolution fusion | flops 1610612736 | bytes 7340032 | tf_op jit(solution)/shard_map/jrd,jdf->jrf/dot_general | solution.py:134
  143.7 40.3 %all-gather.11.cloned.1.call-done = bf16[1,2048,1024]{2,1,0:T(8,128)(2,1)} async-done(((bf16[1,2048,128]{2,1,0:T(8,128)(2,1)}), bf16[1,2048,1024]{2,1,0:T(8,128)(2,1)}) %all-gather.11.cloned.1.call-update) | async-done | bytes 4194320 | tf_op jit(solution)/shard_map/all_gather | solution.py:133
  184.0 5.0 %multiply_convert_fusion = bf16[384,1024]{1,0:T(8,128)(2,1)S(1)} fusion(f32[384,1024]{1,0:T(8,128)} %fusion.22, bf16[384,2048]{1,0:T(8,128)(2,1)} %bitcast.12, bf16[1,2048,1024]{2,1,0:T(8,128)(2,1)} %all-gather.11.cloned.1.call-done), kind=kOutput, calls=%fused_computation.41 | convolution fusion | flops 1612972032 | bytes 8126464 | tf_op jit(solution)/shard_map/jrd,jdf->jrf/dot_general | solution.py:137
  191.9 1.7 fusion.34
  196.3 2.5 %add_convert_fusion = bf16[384,2048]{1,0:T(8,128)(2,1)} fusion(f32[384,2048]{1,0:T(8,128)S(1)} %fusion.30, f32[384,2048]{1,0:T(8,128)S(1)} %fusion.32, f32[384,2048]{1,0:T(8,128)S(1)} %fusion.34, f32[384,2048]{1,0:T(8,128)S(1)} %fusion.36, f32[384,2048]{1,0:T(8,128)S(1)} %fusion.38, f32[384,2048]{1,0:T(8,128)S(1)} %fusion.42, f32[384,2048]{1,0:T(8,128)S(1)} %fusion.40, ...), kind=kOutput, calls=%fused_computation.39 | convolution fusion | flops 207618048 | bytes 24215556 | tf_op jit(solution)/shard_map/jrf,jdf->jrd/dot_general | solution.py:143
  198.8 3.9 %all-to-all-start.1 = ((bf16[4,96,2048]{2,1,0:T(8,128)(2,1)}), bf16[4,96,2048]{2,1,0:T(8,128)(2,1)S(1)}, u32[]{:S(2)}, u32[]{:S(2)}) async-start(bf16[4,96,2048]{2,1,0:T(8,128)(2,1)} %bitcast.79), calls=%async_computation.2 | async-start | bytes 3145728 | tf_op jit(solution)/shard_map/all_to_all | solution.py:154
  202.9 19.6 %all-to-all-done.1 = bf16[4,96,2048]{2,1,0:T(8,128)(2,1)S(1)} async-done(((bf16[4,96,2048]{2,1,0:T(8,128)(2,1)}), bf16[4,96,2048]{2,1,0:T(8,128)(2,1)S(1)}, u32[]{:S(2)}, u32[]{:S(2)}) %all-to-all-start.1) | async-done | bytes 1572896 | tf_op jit(solution)/shard_map/all_to_all | solution.py:154
  222.5 2.3 gather_fusion.1
  224.8 2.4 reshape.227
  227.2 3.9 %multiply_reduce_fusion = bf16[128,2048]{1,0:T(8,128)(2,1)} fusion(f32[128,2,2048]{2,1,0:T(2,128)S(1)} %reshape.227, f32[128,2]{1,0:T(8,128)S(1)} %copy.29), kind=kLoop, calls=%fused_computation.40 | loop fusion | flops 786432 | bytes 2622464 | tf_op jit(solution)/shard_map/reduce_sum | solution.py:159
  (127 shorter events, 22.2 us)
Async XLA Ops:
  7.2 82.1 %copy-start = (bf16[2,128,2048]{2,1,0:T(8,128)(2,1)S(1)}, bf16[2,128,2048]{2,1,0:T(8,128)(2,1)}, u32[]{:S(2)}) copy-start(bf16[2,128,2048]{2,1,0:T(8,128)(2,1)} %param.23) | copy-start | bytes 3145732
  7.2 5.5 %copy-start.12 = (s32[128,2]{0,1:T(2,128)S(1)}, s32[128,2]{0,1:T(2,128)}, u32[]{:S(2)}) copy-start(s32[128,2]{0,1:T(2,128)} %param.26) | copy-start | bytes 3076
  7.2 5.8 %copy-start.1 = (bf16[128,2048]{1,0:T(8,128)(2,1)S(1)}, bf16[128,2048]{1,0:T(8,128)(2,1)}, u32[]{:S(2)}) copy-start(bf16[128,2048]{1,0:T(8,128)(2,1)} %param.24) | copy-start | bytes 1572868
  7.2 18.4 %copy-start.11 = (f32[2048]{0:T(1024)S(1)}, f32[2048]{0:T(1024)}, u32[]{:S(2)}) copy-start(f32[2048]{0:T(1024)} %param.25) | copy-start | bytes 24580
  7.2 48.0 %all-gather.5.cloned.1.call-start = ((), (), s32[]{:S(2)}) async-start(), calls=%async_computation.3 | async-start | bytes 1310720 | tf_op jit(solution)/shard_map/all_gather | solution.py:65
  9.1 68.3 %all-gather.7.cloned.1.call-start = ((), (), s32[]{:S(2)}) async-start(), calls=%async_computation.4 | async-start | bytes 1310720 | tf_op jit(solution)/shard_map/all_gather | solution.py:66
  10.9 127.2 %all-gather.9.cloned.1.call-start = ((), (), s32[]{:S(2)}) async-start(), calls=%async_computation.6 | async-start | bytes 4718592 | tf_op jit(solution)/shard_map/all_gather | solution.py:132
  11.6 172.4 %all-gather.11.cloned.1.call-start = ((), (), s32[]{:S(2)}) async-start(), calls=%async_computation.7 | async-start | bytes 4718592 | tf_op jit(solution)/shard_map/all_gather | solution.py:133
  12.2 11.4 %collective-permute-start = (bf16[1,2048,128]{2,1,0:T(8,128)(2,1)S(1)}, bf16[1,2048,128]{2,1,0:T(8,128)(2,1)S(1)}, u32[]{:S(2)}, u32[]{:S(2)}) collective-permute-start(bf16[1,2048,128]{2,1,0:T(8,128)(2,1)S(1)} %copy-done.2), channel_id=1, source_target_pairs={{0,1},{1,2},{2,3},{3,4},{4,5},{5,6},{6,7},{7,0},{8,9},{9,10},{10,1... | collective-permute-start | bytes 1572872 | tf_op jit(solution)/shard_map/ppermute | solution.py:15
  23.6 25.4 %copy-start.4 = (bf16[1,2048,128]{2,1,0:T(8,128)(2,1)}, bf16[1,2048,128]{2,1,0:T(8,128)(2,1)S(1)}, u32[]{:S(2)}) copy-start(bf16[1,2048,128]{2,1,0:T(8,128)(2,1)S(1)} %collective-permute-done) | copy-start | bytes 1572868
  23.6 10.4 %collective-permute-start.1 = (bf16[1,2048,128]{2,1,0:T(8,128)(2,1)S(1)}, bf16[1,2048,128]{2,1,0:T(8,128)(2,1)S(1)}, u32[]{:S(2)}, u32[]{:S(2)}) collective-permute-start(bf16[1,2048,128]{2,1,0:T(8,128)(2,1)S(1)} %collective-permute-done), channel_id=1, source_target_pairs={{0,1},{1,2},{2,3},{3,4},{4,5},{5,6},{6,7},{7,0},{8,9},{9,10},{10,1... | collective-permute-start | bytes 1572872 | tf_op jit(solution)/shard_map/ppermute | solution.py:15
  34.0 15.0 %copy-start.6 = (bf16[1,2048,128]{2,1,0:T(8,128)(2,1)}, bf16[1,2048,128]{2,1,0:T(8,128)(2,1)S(1)}, u32[]{:S(2)}) copy-start(bf16[1,2048,128]{2,1,0:T(8,128)(2,1)S(1)} %collective-permute-done.1) | copy-start | bytes 1572868
  34.0 10.4 %collective-permute-start.2 = (bf16[1,2048,128]{2,1,0:T(8,128)(2,1)S(1)}, bf16[1,2048,128]{2,1,0:T(8,128)(2,1)S(1)}, u32[]{:S(2)}, u32[]{:S(2)}) collective-permute-start(bf16[1,2048,128]{2,1,0:T(8,128)(2,1)S(1)} %collective-permute-done.1), channel_id=1, source_target_pairs={{0,1},{1,2},{2,3},{3,4},{4,5},{5,6},{6,7},{7,0},{8,9},{9,10},{10,1... | collective-permute-start | bytes 1572872 | tf_op jit(solution)/shard_map/ppermute | solution.py:15
  44.4 10.5 %collective-permute-start.3 = (bf16[1,2048,128]{2,1,0:T(8,128)(2,1)S(1)}, bf16[1,2048,128]{2,1,0:T(8,128)(2,1)}, u32[]{:S(2)}, u32[]{:S(2)}) collective-permute-start(bf16[1,2048,128]{2,1,0:T(8,128)(2,1)S(1)} %collective-permute-done.2), channel_id=1, source_target_pairs={{0,1},{1,2},{2,3},{3,4},{4,5},{5,6},{6,7},{7,0},{8,9},{9,10},{10,1... | collective-permute-start | bytes 1572872 | tf_op jit(solution)/shard_map/ppermute | solution.py:15
  49.0 5.9 %copy-start.10 = (bf16[512,2,128]{2,1,0:T(2,128)(2,1)S(1)}, bf16[512,2,128]{2,1,0:T(2,128)(2,1)}, u32[]{:S(2)}) copy-start(bf16[512,2,128]{2,1,0:T(2,128)(2,1)} %param.18) | copy-start | bytes 786436
  49.0 62.2 %all-to-all-start = ((bf16[4,96,2048]{2,1,0:T(8,128)(2,1)}), bf16[4,96,2048]{2,1,0:T(8,128)(2,1)}, u32[]{:S(2)}, u32[]{:S(2)}) async-start(bf16[4,96,2048]{2,1,0:T(8,128)(2,1)} %bitcast.11), calls=%async_computation.1 | async-start | bytes 3145728 | tf_op jit(solution)/shard_map/all_to_all | solution.py:127
  53.6 177.5 %reduce-scatter.2.cloned.1.call-start = ((), (), s32[]{:S(2)}) async-start(), calls=%async_computation.5 | async-start | bytes 2359296 | tf_op jit(solution)/shard_map/reduce_scatter | solution.py:93
  55.0 34.2 %collective-permute-start.4 = (bf16[1,2048,128]{2,1,0:T(8,128)(2,1)}, bf16[1,2048,128]{2,1,0:T(8,128)(2,1)}, u32[]{:S(2)}, u32[]{:S(2)}) collective-permute-start(bf16[1,2048,128]{2,1,0:T(8,128)(2,1)} %collective-permute-done.3), channel_id=1, source_target_pairs={{0,1},{1,2},{2,3},{3,4},{4,5},{5,6},{6,7},{7,0},{8,9},{9,10},{10,1... | collective-permute-start | bytes 1572872 | tf_op jit(solution)/shard_map/ppermute | solution.py:15
  78.8 9.9 %copy-start.14 = (f32[2]{0:T(128)S(1)}, f32[2]{0:T(128)}, u32[]{:S(2)}) copy-start(f32[2]{0:T(128)} %param.21) | copy-start | bytes 28
  78.8 10.5 %copy-start.15 = (f32[128]{0:T(128)S(1)}, f32[128]{0:T(128)}, u32[]{:S(2)}) copy-start(f32[128]{0:T(128)} %param.22) | copy-start | bytes 1540
  89.2 22.0 %collective-permute-start.5 = (bf16[1,2048,128]{2,1,0:T(8,128)(2,1)}, bf16[1,2048,128]{2,1,0:T(8,128)(2,1)S(1)}, u32[]{:S(2)}, u32[]{:S(2)}) collective-permute-start(bf16[1,2048,128]{2,1,0:T(8,128)(2,1)} %collective-permute-done.4), channel_id=1, source_target_pairs={{0,1},{1,2},{2,3},{3,4},{4,5},{5,6},{6,7},{7,0},{8,9},{9,10},{10,1... | collective-permute-start | bytes 1572872 | tf_op jit(solution)/shard_map/ppermute | solution.py:15
  111.2 85.1 %collective-permute-start.6 = (bf16[1,2048,128]{2,1,0:T(8,128)(2,1)S(1)}, bf16[1,2048,128]{2,1,0:T(8,128)(2,1)S(1)}, u32[]{:S(2)}, u32[]{:S(2)}) collective-permute-start(bf16[1,2048,128]{2,1,0:T(8,128)(2,1)S(1)} %collective-permute-done.5), channel_id=1, source_target_pairs={{0,1},{1,2},{2,3},{3,4},{4,5},{5,6},{6,7},{7,0},{8,9},{9,10},{10,1... | collective-permute-start | bytes 1572872 | tf_op jit(solution)/shard_map/ppermute | solution.py:15
  143.7 45.4 %copy-start.3 = (bf16[1,2048,128]{2,1,0:T(8,128)(2,1)S(1)}, bf16[1,2048,128]{2,1,0:T(8,128)(2,1)}, u32[]{:S(2)}) copy-start(bf16[1,2048,128]{2,1,0:T(8,128)(2,1)} %param.31) | copy-start | bytes 1572868
  198.8 23.7 %all-to-all-start.1 = ((bf16[4,96,2048]{2,1,0:T(8,128)(2,1)}), bf16[4,96,2048]{2,1,0:T(8,128)(2,1)S(1)}, u32[]{:S(2)}, u32[]{:S(2)}) async-start(bf16[4,96,2048]{2,1,0:T(8,128)(2,1)} %bitcast.79), calls=%async_computation.2 | async-start | bytes 3145728 | tf_op jit(solution)/shard_map/all_to_all | solution.py:154
  (7 other events, 21.2 us)
Sparse Core Ops, SparseCore 0:
  10.5 29.2 all-gather.4
  41.6 35.7 all-gather.6
  79.0 59.0 all-gather.8
  139.5 44.5 all-gather.10
  186.7 34.1 reduce-scatter.1
